TPU v7x, 32 devices: a whole 2x2x4 slice. The times are simulated.
32 devices in a mesh: sp: 8 (over z, core), tp: 4 (over y, x).
Axes of the slice: x: 2, y: 2, z: 4, core: 2. Of those that a mesh axis runs over, the one named last changes fastest.
Arguments:
- residual_in: bfloat16 [1024, 2048], P('sp'), may hold values from -6 to 6
- queries: bfloat16 [1024, 2048], P('sp', 'tp'), may hold values from -6 to 6
- keys: bfloat16 [1024, 2048], P('sp', 'tp'), may hold values from -6 to 6
- values: bfloat16 [1024, 2048], P('sp', 'tp'), may hold values from -6 to 6
- out_gate: bfloat16 [1024, 2048], P('sp', 'tp'), may hold values from -6 to 6
- beta_logit: bfloat16 [16, 1024], P('tp', 'sp'), may hold values from -6 to -2
- decay_logit: bfloat16 [16, 1024], P('tp', 'sp'), may hold values from -4.5 to 4.5
- decay_log: float32 [16], P('tp'), may hold values from -11 to -3.2
- head_gain: float32 [128], replicated, may hold values from 0.1 to 1.9
- out_weight: bfloat16 [2048, 2048], P('tp'), may hold values from -0.125 to 0.125
- norm_gain: float32 [2048], replicated, may hold values from 0.1 to 1.9
- final_gain: float32 [2048], replicated, may hold values from 0.1 to 1.9
- expert_index: int32 [1024, 2], P('sp'), may hold values from 0 to 7, all different within a row; in each aligned block of 32 rows (0 to 31, 32 to 63, ...) at most 16 rows name the same one
- route_weights: float32 [1024, 2], P('sp'), may hold values from 0.2 to 1
- expert_gate: bfloat16 [8, 2048, 6144], P('sp', None, 'tp'), may hold values from -0.125 to 0.125
- expert_up: bfloat16 [8, 2048, 6144], P('sp', None, 'tp'), may hold values from -0.125 to 0.125
- expert_down: bfloat16 [8, 6144, 2048], P('sp', 'tp'), may hold values from -0.078125 to 0.078125
Outputs:
- layer_out: bfloat16 [1024, 2048], P('sp')
Inputs may be any that keep to these rules, and one draw needn't show every extreme that they name: `expert_index`: in each aligned block of 32 rows no expert is named by more than 16 rows, a bound that some block reaches; a row names 2 different experts.
All inputs are finite; a program needn't handle non-finite values.
Results may differ from a plain program's by a relative error of at most 0.015.
Values may be sent and summed in bfloat16 or wider, within the bound.
A program may use at most 64 MiB of HBM per device.

v0:
```python
import functools

import jax
import jax.numpy as jnp
from jax import lax
from jax.experimental import pallas as pl
from jax.experimental.pallas import tpu as pltpu
from jax.sharding import PartitionSpec as P

MESH = pl.DeviceIdType.MESH

HEAD_FEATURES = 128
TOP = 2
BLOCK = 64
GROUP = 2


highest_precision = lax.Precision.HIGHEST
residual_scale = 2.0**0.5


def carried_in(x, axis, join, neutral):
    place = lax.axis_index(axis)
    gathered = jax.tree.map(
        lambda a, kind: lax.all_gather(a.astype(kind), axis), x, (jnp.bfloat16, jnp.bfloat16)
    )
    state = jax.tree.map(lambda a, e: jnp.zeros_like(a) + jnp.asarray(e, a.dtype), x, neutral)

    def one(turn, state):
        return join(
            state,
            jax.tree.map(
                lambda a, own: lax.dynamic_index_in_dim(a, turn, 0, False).astype(own.dtype),
                gathered,
                x,
            ),
        )

    return lax.fori_loop(0, place, one, state)


def unit_rows(data):
    return data * lax.rsqrt(jnp.sum(data * data, -1, keepdims=True) + 1e-06)


def layer_norm(data, gain):
    center = data - jnp.mean(data, -1, keepdims=True)
    return center * lax.rsqrt(jnp.mean(center * center, -1, keepdims=True) + 1e-05) * gain


def block_terms(query, key, beta, decay):
    heads, length, width = query.shape
    count = length // BLOCK
    shape = (heads, count, BLOCK, width)
    query = query.reshape(shape)
    key = key.reshape(shape)
    beta = beta.reshape(heads, count, BLOCK)
    running = jnp.cumsum(decay.reshape(heads, count, BLOCK), axis=-1)
    causal = jnp.tril(jnp.ones((BLOCK, BLOCK), bool))
    strict = jnp.tril(jnp.ones((BLOCK, BLOCK), bool), -1)
    within = jnp.exp(jnp.where(causal, running[..., :, None] - running[..., None, :], -jnp.inf))
    key_beta = key * beta[..., None]
    lower = jnp.where(
        strict,
        jnp.einsum("hnid,hnjd->hnij", key_beta, key, precision=highest_precision) * within,
        0.0,
    )
    system = jnp.eye(BLOCK, dtype=jnp.float32) + lower
    weighted = jax.scipy.linalg.solve_triangular(
        system, key_beta * jnp.exp(running)[..., None], lower=True, unit_diagonal=True
    )
    scores = jnp.einsum("hnid,hnjd->hnij", query, key, precision=highest_precision) * within
    query_decayed = query * jnp.exp(running)[..., None]
    key_decayed = key * jnp.exp(running[..., -1:] - running)[..., None]
    block_decay = jnp.exp(running[..., -1])
    return (system, beta, weighted, query_decayed, key_decayed, scores, block_decay)


def run_blocks(terms, value, start):
    system, beta, weighted, query_decayed, key_decayed, scores, block_decay = terms
    heads, count = (beta.shape[0], beta.shape[1])
    fresh = jax.scipy.linalg.solve_triangular(
        system,
        value.reshape(heads, count, BLOCK, -1) * beta[..., None],
        lower=True,
        unit_diagonal=True,
    )
    missing = start.shape[-1] - fresh.shape[-1]
    fresh = jnp.concatenate([fresh, jnp.zeros(fresh.shape[:-1] + (missing,), jnp.float32)], -1)

    def advance(recurrent_state, inputs):
        (
            fresh_value_block,
            block_weighted_values,
            block_queries,
            block_keys,
            block_scores,
            block_decay_factor,
        ) = inputs
        corrected_value = fresh_value_block - jnp.einsum(
            "nya,nag->nyg", block_weighted_values, recurrent_state, precision=highest_precision
        )
        state_next = block_decay_factor[:, None, None] * recurrent_state + jnp.einsum(
            "iyp,iyu->ipu", block_keys, corrected_value, precision=highest_precision
        )
        final_output = jnp.einsum(
            "nya,nag->nyg", block_queries, recurrent_state, precision=highest_precision
        ) + jnp.einsum("emp,epk->emk", block_scores, corrected_value, precision=highest_precision)
        return (state_next, final_output)

    inputs = tuple(
        (
            jnp.moveaxis(item, 1, 0)
            for item in (fresh, weighted, query_decayed, key_decayed, scores, block_decay)
        )
    )
    final, output_list = lax.scan(advance, start, inputs)
    return (jnp.moveaxis(output_list, 0, 1).reshape(heads, count * BLOCK, -1), final)


def compose(earlier, later):
    return (
        jnp.einsum("hij,hjk->hik", later[0], earlier[0], precision=highest_precision),
        jnp.einsum("hij,hjk->hik", later[0], earlier[1], precision=highest_precision) + later[1],
    )


def slot_places(routes, groups, capacity, experts):
    rows, picks = routes.shape
    flat = routes.reshape(groups, rows // groups * picks)
    matches = (flat[..., None] == jnp.arange(experts, dtype=jnp.int32)).astype(jnp.int32)
    before = jnp.cumsum(matches, axis=1) - matches
    rank = jnp.sum(before * matches, -1)
    group = jnp.arange(groups, dtype=jnp.int32)[:, None]
    return ((flat * groups + group) * capacity + rank).reshape(rows, picks)


def per_device(
    residual_in,
    queries,
    keys,
    values,
    out_gate,
    beta_logit,
    decay_logit,
    decay_log,
    head_gain,
    out_weight,
    norm_gain,
    final_gain,
    expert_index,
    route_weights,
    expert_gate,
    expert_up,
    expert_down,
):
    length, width = residual_in.shape
    heads = beta_logit.shape[0]

    def split_heads(data):
        return data.astype(jnp.float32).reshape(length, heads, HEAD_FEATURES).transpose(1, 0, 2)

    query = unit_rows(split_heads(queries)) * HEAD_FEATURES ** (-0.5)
    key = unit_rows(split_heads(keys))
    value = split_heads(values)
    beta = jax.nn.sigmoid(beta_logit.astype(jnp.float32))
    decay = -jnp.exp(decay_log)[:, None] * jax.nn.softplus(decay_logit.astype(jnp.float32))
    terms = block_terms(query, key, beta, decay)
    identity_map = jnp.broadcast_to(
        jnp.eye(HEAD_FEATURES, dtype=jnp.float32), (heads, HEAD_FEATURES, HEAD_FEATURES)
    )
    blank = jnp.zeros((heads, HEAD_FEATURES, HEAD_FEATURES), jnp.float32)
    extended = jnp.concatenate([blank, identity_map], -1)
    output_list, final = run_blocks(terms, value, extended)
    prefix = carried_in(
        (final[..., HEAD_FEATURES:], final[..., :HEAD_FEATURES]),
        "sp",
        compose,
        (identity_map, blank),
    )
    entry_value = prefix[1]
    mixed = output_list[..., :HEAD_FEATURES] + jnp.einsum(
        "apj,ajz->apz", output_list[..., HEAD_FEATURES:], entry_value, precision=highest_precision
    )
    normalized = mixed * lax.rsqrt(jnp.mean(mixed * mixed, -1, keepdims=True) + 1e-06) * head_gain
    gated = (
        (normalized * jax.nn.silu(split_heads(out_gate)))
        .transpose(1, 0, 2)
        .reshape(length, heads * HEAD_FEATURES)
        .astype(jnp.bfloat16)
    )
    split_count = lax.axis_size("tp")
    expert_count = lax.axis_size("sp") * expert_gate.shape[0]
    rows = length // split_count
    first = lax.axis_index("tp") * rows
    projected = lax.psum_scatter(
        jnp.dot(gated, out_weight, preferred_element_type=jnp.float32).astype(jnp.bfloat16),
        "tp",
        scatter_dimension=0,
        tiled=True,
    ).astype(jnp.float32)
    residual = lax.dynamic_slice_in_dim(residual_in, first, rows, 0)
    routes = lax.dynamic_slice_in_dim(expert_index, first, rows, 0)
    weights = lax.dynamic_slice_in_dim(route_weights, first, rows, 0)
    groups = 1
    capacity = 2 * TOP * (length // split_count) // expert_count
    hidden_in = layer_norm(
        residual_scale * residual.astype(jnp.float32) + projected, norm_gain
    ).astype(jnp.bfloat16)
    places = slot_places(routes, groups, capacity, expert_count)
    slots = expert_count * groups * capacity
    table = (places[:, :, None] == jnp.arange(slots, dtype=jnp.int32)).astype(jnp.bfloat16)
    send = jnp.einsum(
        "rs,rd->sd", jnp.sum(table, 1), hidden_in, preferred_element_type=jnp.float32
    ).astype(jnp.bfloat16)
    arrived = lax.all_to_all(
        send.reshape(expert_count, groups * capacity, width),
        "sp",
        split_axis=0,
        concat_axis=0,
        tiled=True,
    ).reshape(slots, width)
    gate_matrix, up_matrix, down_matrix = (expert_gate[0], expert_up[0], expert_down[0])
    piece = lax.all_gather(arrived, "tp", axis=0, tiled=True)
    gate = jnp.dot(piece, gate_matrix, preferred_element_type=jnp.float32)
    up = jnp.dot(piece, up_matrix, preferred_element_type=jnp.float32)
    inner = (jax.nn.silu(gate) * up).astype(jnp.bfloat16)
    partial_value = jnp.dot(inner, down_matrix, preferred_element_type=jnp.float32)
    result = lax.psum_scatter(
        partial_value.astype(jnp.bfloat16), "tp", scatter_dimension=0, tiled=True
    )
    back = lax.all_to_all(
        result.reshape(expert_count, groups * capacity, width),
        "sp",
        split_axis=0,
        concat_axis=0,
        tiled=True,
    ).reshape(slots, width)
    gathered = jnp.einsum("rks,sd->rkd", table, back, preferred_element_type=jnp.float32)
    routed = jnp.sum(weights[..., None] * gathered, 1)
    layer_out = layer_norm(
        residual_scale * hidden_in.astype(jnp.float32) + routed, final_gain
    ).astype(jnp.bfloat16)
    layer_out = lax.all_gather(layer_out, "tp", axis=0, tiled=True)
    return layer_out


def mm(a, b):
    return jnp.dot(a.astype(jnp.bfloat16), b.astype(jnp.bfloat16), preferred_element_type=jnp.float32)


def mm_nt(a, b):
    return lax.dot_general(
        a.astype(jnp.bfloat16),
        b.astype(jnp.bfloat16),
        (((1,), (1,)), ((), ())),
        preferred_element_type=jnp.float32,
    )


def mm_tn(a, b):
    return lax.dot_general(
        a.astype(jnp.bfloat16),
        b.astype(jnp.bfloat16),
        (((0,), (0,)), ((), ())),
        preferred_element_type=jnp.float32,
    )


def layer_kernel(
    n_sp,
    n_tp,
    residual_ref,
    query_ref,
    key_ref,
    value_ref,
    out_gate_ref,
    beta_ref,
    decay_ref,
    decay_log_ref,
    head_gain_ref,
    norm_gain_ref,
    final_gain_ref,
    index_ref,
    weights_ref,
    out_weight_hbm,
    gate_hbm,
    up_hbm,
    down_hbm,
    out_ref,
    out_weight_v,
    gate_v,
    up_v,
    down_v,
    maps_v,
    adds_v,
    state_in,
    state_out,
    mixed_v,
    readout_v,
    gated_v,
    proj_v,
    proj_in,
    hidden_v,
    send_v,
    arrived_v,
    inner_v,
    part_v,
    part_in,
    pair_v,
    result_v,
    back_v,
    local_sem,
    state_sem,
    proj_sem,
    send_sem,
    fan_sem,
    part_sem,
    back_sem,
    out_sem,
):
    s = lax.axis_index("sp")
    t = lax.axis_index("tp")
    length, width = residual_ref.shape
    heads = beta_ref.shape[0]
    rows = length // n_tp
    chunks, _, group, cap, _ = arrived_v.shape
    half = width // 2
    right, left = slice(half, width), slice(0, half)
    slots = n_sp * cap
    feat = HEAD_FEATURES
    hidden_units = gate_v.shape[1]

    local = [
        pltpu.make_async_copy(out_weight_hbm, out_weight_v, local_sem.at[0]),
        pltpu.make_async_copy(gate_hbm.at[0], gate_v, local_sem.at[1]),
        pltpu.make_async_copy(up_hbm.at[0], up_v, local_sem.at[2]),
        pltpu.make_async_copy(down_hbm.at[0], down_v, local_sem.at[3]),
    ]
    for copy in local:
        copy.start()

    barrier = pltpu.get_barrier_semaphore()
    for k in range(1, n_sp):
        pl.semaphore_signal(
            barrier, inc=1, device_id=(lax.rem(s + k, n_sp), t), device_id_type=MESH
        )
    for k in range(1, n_tp):
        pl.semaphore_signal(
            barrier, inc=1, device_id=(s, lax.rem(t + k, n_tp)), device_id_type=MESH
        )

    def remote(src, dst, sem_a, sem_b, to_s, to_t):
        return pltpu.make_async_remote_copy(
            src_ref=src,
            dst_ref=dst,
            send_sem=sem_a,
            recv_sem=sem_b,
            device_id=(to_s, to_t),
            device_id_type=MESH,
        )

    row_id = lax.broadcasted_iota(jnp.int32, (length, length), 0)
    col_id = lax.broadcasted_iota(jnp.int32, (length, length), 1)
    causal = row_id >= col_id
    strict = row_id > col_id
    eye = (row_id == col_id).astype(jnp.float32)
    tril = causal.astype(jnp.float32)
    beta = jax.nn.sigmoid(beta_ref[...].astype(jnp.float32))
    logit = decay_ref[...].astype(jnp.float32)
    soft = jnp.maximum(logit, 0.0) + jnp.log(1.0 + jnp.exp(-jnp.abs(logit)))
    head_eye = lax.broadcasted_iota(jnp.int32, (heads, heads), 0) == lax.broadcasted_iota(
        jnp.int32, (heads, heads), 1
    )
    rate = jnp.sum(jnp.where(head_eye, jnp.exp(decay_log_ref[...]), 0.0), 1, keepdims=True)
    decay = -rate * soft
    exact = functools.partial(
        lax.dot_general, precision=highest_precision, preferred_element_type=jnp.float32
    )
    nt = (((1,), (1,)), ((), ()))
    run_rows = exact(decay, tril, nt)
    run_cols = exact(tril, decay, nt)
    beta_cols = exact(eye, beta, nt)

    lowers, inverses, rights, score_list, q_list, kd_list, last_list = [], [], [], [], [], [], []
    for h in range(heads):
        cols = slice(h * feat, (h + 1) * feat)
        query = unit_rows(query_ref[:, cols].astype(jnp.float32)) * feat ** (-0.5)
        key = unit_rows(key_ref[:, cols].astype(jnp.float32))
        value = value_ref[:, cols].astype(jnp.float32)
        run_c = run_cols[:, h : h + 1]
        run_r = run_rows[h : h + 1, :]
        beta_c = beta_cols[:, h : h + 1]
        last = run_cols[length - 1 : length, h : h + 1]
        within = jnp.where(causal, jnp.exp(jnp.minimum(run_c - run_r, 0.0)), 0.0)
        lowers.append(jnp.where(strict, mm_nt(key, key) * within * beta_c, 0.0))
        score_list.append((mm_nt(query, key) * within).astype(jnp.bfloat16))
        grown = jnp.exp(run_c)
        rights.append(
            jnp.concatenate([value * beta_c, key * (beta_c * grown)], 1).astype(jnp.bfloat16)
        )
        q_list.append(query * grown)
        kd_list.append((key * jnp.exp(last - run_c)).astype(jnp.bfloat16))
        last_list.append(jnp.exp(last))

    def level(size):
        mid = size // 2
        return (row_id // size == col_id // size) & (row_id % size >= mid) & (col_id % size < mid)

    first = level(2)
    inverses = [eye - jnp.where(first, low, 0.0) for low in lowers]
    size = 4
    while size <= length:
        mask = level(size)
        steps = [mm(jnp.where(mask, low, 0.0), inv) for low, inv in zip(lowers, inverses)]
        inverses = [inv - mm(inv, step) for inv, step in zip(inverses, steps)]
        size *= 2
    solved = [mm(inv, right).astype(jnp.bfloat16) for inv, right in zip(inverses, rights)]
    for h in range(heads):
        ends = mm_tn(kd_list[h], solved[h])
        adds_v[h] = ends[:, :feat]
        maps_v[h] = (last_list[h] * eye[:feat, :feat] - ends[:, feat:]).astype(jnp.bfloat16)
    for h in range(heads):
        seen = mm(score_list[h], solved[h])
        mixed_v[h] = seen[:, :feat]
        readout_v[h] = (q_list[h] - seen[:, feat:]).astype(jnp.bfloat16)

    pl.semaphore_wait(barrier, n_sp - 1 + n_tp - 1)

    after = lax.rem(s + 1, n_sp)

    def state_copy(h):
        return remote(
            state_out.at[h], state_in.at[h], state_sem.at[0, h], state_sem.at[1, h], after, t
        )

    @pl.when(s == 0)
    def _():
        state_in[...] = jnp.zeros_like(state_in)

    for h in range(heads):

        @pl.when(s > 0)
        def _():
            state_copy(h).wait_recv()

        @pl.when(s < n_sp - 1)
        def _():
            state_out[h] = (mm(maps_v[h], state_in[h]) + adds_v[h]).astype(jnp.bfloat16)
            state_copy(h).start()

    for h in range(heads):
        cols = slice(h * feat, (h + 1) * feat)
        mixed = mixed_v[h] + mm(readout_v[h], state_in[h])
        normalized = (
            mixed * lax.rsqrt(jnp.mean(mixed * mixed, -1, keepdims=True) + 1e-06) * head_gain_ref[...]
        )
        gate = out_gate_ref[:, cols].astype(jnp.float32)
        gated_v[:, cols] = (normalized * (gate * jax.nn.sigmoid(gate))).astype(jnp.bfloat16)

    local[0].wait()

    def project(i, carry):
        cols = pl.ds(pl.multiple_of(i * 512, 512), 512)
        proj_v[:, cols] = jnp.dot(
            gated_v[...], out_weight_v[:, cols], preferred_element_type=jnp.float32
        ).astype(jnp.bfloat16)
        return carry

    lax.fori_loop(0, width // 512, project, 0)

    def row_block(i):
        return pl.ds(pl.multiple_of(i * rows, rows), rows)

    proj_copies = []
    for k in range(1, n_tp):
        to = lax.rem(t + k, n_tp)
        copy = remote(
            proj_v.at[row_block(to)], proj_in.at[k - 1], proj_sem.at[0, k - 1], proj_sem.at[1, k - 1], s, to
        )
        copy.start()
        proj_copies.append(copy)

    own_row = (
        lax.broadcasted_iota(jnp.int32, (rows, length), 1)
        == lax.broadcasted_iota(jnp.int32, (rows, length), 0) + t * rows
    ).astype(jnp.float32)
    index = exact(own_row, index_ref[...].astype(jnp.float32), nt)
    weights = exact(own_row, weights_ref[...], nt)
    slot_id = lax.broadcasted_iota(jnp.int32, (rows, slots), 1)
    owner = (slot_id // cap).astype(jnp.float32)
    picks = [(index[:, j : j + 1] == owner).astype(jnp.float32) for j in range(TOP)]
    both = functools.reduce(jnp.add, picks)
    earlier = (
        lax.broadcasted_iota(jnp.int32, (rows, rows), 0)
        > lax.broadcasted_iota(jnp.int32, (rows, rows), 1)
    ).astype(jnp.float32)
    rank = mm(earlier, both)
    here = (rank == (slot_id % cap).astype(jnp.float32)).astype(jnp.float32)
    tables = [(pick * here).astype(jnp.bfloat16) for pick in picks]
    table = (both * here).astype(jnp.bfloat16)

    tx = t + 1 - 2 * lax.rem(t, 2)
    ty = lax.rem(t + 2, 4)
    td = lax.rem(tx + 2, 4)

    def send_copy(to):
        return remote(
            send_v.at[to],
            arrived_v.at[s // group, t, s % group],
            send_sem.at[0, to],
            send_sem.at[1, s],
            to,
            t,
        )

    def arrival(p):
        return remote(
            send_v.at[p],
            arrived_v.at[p // group, t, p % group],
            send_sem.at[0, p],
            send_sem.at[1, p],
            p,
            t,
        )

    def fan_copies(c):
        mine = arrived_v.at[c, t]
        return [
            remote(mine, mine, fan_sem.at[0, 0, c], fan_sem.at[0, 1, c], s, tx),
            remote(mine, mine, fan_sem.at[1, 0, c], fan_sem.at[1, 1, c], s, ty),
        ]

    def relay_copies(c):
        a = arrived_v.at[c, tx, :, :, left]
        b = arrived_v.at[c, ty, :, :, right]
        return [
            remote(a, a, fan_sem.at[2, 0, c], fan_sem.at[2, 1, c], s, ty),
            remote(b, b, fan_sem.at[3, 0, c], fan_sem.at[3, 1, c], s, tx),
        ]

    def fan_out(c):
        for p in range(c * group, (c + 1) * group):

            @pl.when(s != p)
            def _():
                arrival(p).wait_recv()

        for copy in fan_copies(c):
            copy.start()

    def relay(c):
        for copy, onward in zip(fan_copies(c), relay_copies(c)):
            copy.wait_recv()
            onward.start()

    home = s // group

    @pl.when(home >= 2)
    def _():
        fan_out(0)

    projected = proj_v[row_block(t), :].astype(jnp.float32)
    for k in range(1, n_tp):
        proj_copies[k - 1].wait_recv()
        projected = projected + proj_in[k - 1].astype(jnp.float32)
    residual = residual_ref[row_block(t), :].astype(jnp.float32)
    hidden_in = layer_norm(residual_scale * residual + projected, norm_gain_ref[...]).astype(
        jnp.bfloat16
    )
    hidden_v[...] = hidden_in

    send_v[...] = mm_tn(table, hidden_in).astype(jnp.bfloat16).reshape(n_sp, cap, width)

    for k in range(1, n_sp):
        send_copy(lax.rem(s + k, n_sp)).start()
    arrived_v[home, t, s % group] = send_v[s]

    def part_copies(c):
        def one(kind, src, to):
            return remote(
                src, part_in.at[kind, c], part_sem.at[kind, 0, c], part_sem.at[kind, 1, c], s, to
            )

        return [
            one(0, part_v.at[c, td, :, left], tx),
            one(1, part_v.at[c, td, :, right], ty),
            one(2, part_v.at[c, tx, :, left], tx),
            one(3, part_v.at[c, ty, :, right], ty),
            one(4, pair_v.at[0, c], ty),
            one(5, pair_v.at[1, c], tx),
        ]

    def gate_up(c):
        piece = arrived_v[c].reshape(n_tp * group * cap, width)

        def step(i, carry):
            cols = pl.ds(pl.multiple_of(i * 256, 256), 256)
            gate = jnp.dot(piece, gate_v[:, cols], preferred_element_type=jnp.float32)
            up = jnp.dot(piece, up_v[:, cols], preferred_element_type=jnp.float32)
            inner_v[:, cols] = (gate * jax.nn.sigmoid(gate) * up).astype(jnp.bfloat16)
            return carry

        lax.fori_loop(0, hidden_units // 256, step, 0)

    def down(c):
        def step(i, carry):
            cols = pl.ds(pl.multiple_of(i * 512, 512), 512)
            part_v[c, :, :, cols] = (
                jnp.dot(inner_v[...], down_v[:, cols], preferred_element_type=jnp.float32)
                .astype(jnp.bfloat16)
                .reshape(n_tp, group * cap, 512)
            )
            return carry

        lax.fori_loop(0, width // 512, step, 0)

    def pair_up(c):
        copies = part_copies(c)
        wide = jnp.float32
        copies[0].wait_recv()
        pair_v[0, c] = (part_v[c, ty, :, left].astype(wide) + part_in[0, c].astype(wide)).astype(
            jnp.bfloat16
        )
        copies[4].start()
        copies[1].wait_recv()
        pair_v[1, c] = (part_v[c, tx, :, right].astype(wide) + part_in[1, c].astype(wide)).astype(
            jnp.bfloat16
        )
        copies[5].start()

    def back_copy(c, i):
        return remote(
            result_v.at[c, i],
            back_v.at[s],
            back_sem.at[0, c * group + i],
            back_sem.at[1, s],
            c * group + i,
            t,
        )

    def finish(c):
        copies = part_copies(c)
        for i in range(2, 6):
            copies[i].wait_recv()
        own = part_v[c, t].astype(jnp.float32)
        near, far = part_in[2, c].astype(jnp.float32), part_in[4, c].astype(jnp.float32)
        low = own[:, left] + near + far
        near, far = part_in[3, c].astype(jnp.float32), part_in[5, c].astype(jnp.float32)
        high = own[:, right] + near + far
        result_v[c, :, :, left] = low.astype(jnp.bfloat16).reshape(group, cap, half)
        result_v[c, :, :, right] = high.astype(jnp.bfloat16).reshape(group, cap, half)
        for i in range(group):
            p = c * group + i

            @pl.when(s != p)
            def _():
                back_copy(c, i).start()

            @pl.when(s == p)
            def _():
                back_v[p] = result_v[c, i]

    @pl.when(home < 2)
    def _():
        fan_out(0)

    relay(0)
    if chunks > 1:
        fan_out(1)
    for copy in local[1:]:
        copy.wait()
    for i in range(chunks + 2):
        if i < chunks:
            for copy in relay_copies(i):
                copy.wait_recv()
            gate_up(i)
            if i + 1 < chunks:
                relay(i + 1)
            if i + 2 < chunks:
                fan_out(i + 2)
            down(i)
            for copy in part_copies(i)[:4]:
                copy.start()
        if 1 <= i <= chunks:
            pair_up(i - 1)
        if i >= 2:
            finish(i - 2)

    for p in range(n_sp):

        @pl.when(s != p)
        def _():
            remote(
                result_v.at[0, 0], back_v.at[p], back_sem.at[0, p], back_sem.at[1, p], p, t
            ).wait_recv()

    back = back_v[...].reshape(slots, width)
    routed = jnp.zeros((rows, width), jnp.float32)
    for j in range(TOP):
        routed = routed + weights[:, j : j + 1] * mm(tables[j], back)
    out_ref[row_block(t), :] = layer_norm(
        residual_scale * hidden_v[...].astype(jnp.float32) + routed, final_gain_ref[...]
    ).astype(jnp.bfloat16)

    out_copies = []
    for k in range(1, n_tp):
        copy = remote(
            out_ref.at[row_block(t)],
            out_ref.at[row_block(t)],
            out_sem.at[0, k - 1],
            out_sem.at[1, k - 1],
            s,
            lax.rem(t + k, n_tp),
        )
        copy.start()
        out_copies.append(copy)

    @pl.when(s < n_sp - 1)
    def _():
        for h in range(heads):
            state_copy(h).wait_send()

    for copy in proj_copies:
        copy.wait_send()
    for k in range(1, n_sp):
        send_copy(lax.rem(s + k, n_sp)).wait_send()
    for c in range(chunks):
        for copy in fan_copies(c) + relay_copies(c) + part_copies(c):
            copy.wait_send()
        for i in range(group):

            @pl.when(s != c * group + i)
            def _():
                back_copy(c, i).wait_send()

    for copy in out_copies:
        copy.wait()


def fused(args, n_sp, n_tp, cap):
    (residual_in, queries, keys, values, out_gate, beta_logit, decay_logit, decay_log, head_gain,
     out_weight, norm_gain, final_gain, expert_index, route_weights, expert_gate, expert_up,
     expert_down) = args
    length, width = residual_in.shape
    heads = beta_logit.shape[0]
    rows = length // n_tp
    chunks = n_sp // GROUP
    units = expert_gate.shape[2]
    feat = HEAD_FEATURES
    low, full = jnp.bfloat16, jnp.float32
    vmem = pl.BlockSpec(memory_space=pltpu.VMEM)
    hbm = pl.BlockSpec(memory_space=pl.ANY)
    dma = pltpu.SemaphoreType.DMA
    return pl.pallas_call(
        functools.partial(layer_kernel, n_sp, n_tp),
        out_shape=jax.ShapeDtypeStruct((length, width), low),
        in_specs=[vmem] * 13 + [hbm] * 4,
        out_specs=vmem,
        scratch_shapes=[
            pltpu.VMEM(out_weight.shape, low),
            pltpu.VMEM(expert_gate.shape[1:], low),
            pltpu.VMEM(expert_up.shape[1:], low),
            pltpu.VMEM(expert_down.shape[1:], low),
            pltpu.VMEM((heads, feat, feat), low),
            pltpu.VMEM((heads, feat, feat), full),
            pltpu.VMEM((heads, feat, feat), low),
            pltpu.VMEM((heads, feat, feat), low),
            pltpu.VMEM((heads, length, feat), full),
            pltpu.VMEM((heads, length, feat), low),
            pltpu.VMEM((length, heads * feat), low),
            pltpu.VMEM((length, width), low),
            pltpu.VMEM((n_tp - 1, rows, width), low),
            pltpu.VMEM((rows, width), low),
            pltpu.VMEM((n_sp, cap, width), low),
            pltpu.VMEM((chunks, n_tp, GROUP, cap, width), low),
            pltpu.VMEM((n_tp * GROUP * cap, units), low),
            pltpu.VMEM((chunks, n_tp, GROUP * cap, width), low),
            pltpu.VMEM((6, chunks, GROUP * cap, width // 2), low),
            pltpu.VMEM((2, chunks, GROUP * cap, width // 2), low),
            pltpu.VMEM((chunks, GROUP, cap, width), low),
            pltpu.VMEM((n_sp, cap, width), low),
            dma((4,)),
            dma((2, heads)),
            dma((2, n_tp - 1)),
            dma((2, n_sp)),
            dma((4, 2, chunks)),
            dma((6, 2, chunks)),
            dma((2, n_sp)),
            dma((2, n_tp - 1)),
        ],
        compiler_params=pltpu.CompilerParams(
            collective_id=0, has_side_effects=True, vmem_limit_bytes=60 * 1024 * 1024
        ),
    )(
        residual_in, queries, keys, values, out_gate, beta_logit, decay_logit,
        decay_log.reshape(1, heads), head_gain.reshape(1, -1), norm_gain.reshape(1, -1),
        final_gain.reshape(1, -1), expert_index.T, route_weights.T, out_weight, expert_gate,
        expert_up, expert_down,
    )


def any_size(*args):
    n_sp, n_tp = lax.axis_size("sp"), lax.axis_size("tp")
    residual_in, expert_gate = args[0], args[14]
    length, width = residual_in.shape
    experts = n_sp * expert_gate.shape[0]
    cap = 2 * TOP * (length // n_tp) // experts
    fits = (
        expert_gate.shape[0] == 1
        and n_sp > GROUP
        and n_sp % GROUP == 0
        and n_tp == 4
        and length == HEAD_FEATURES
        and cap % 16 == 0
        and (length // n_tp) % 16 == 0
        and (n_sp * cap) % 128 == 0
        and width % 512 == 0
        and expert_gate.shape[2] % 256 == 0
    )
    return fused(args, n_sp, n_tp, cap) if fits else per_device(*args)


def solution(mesh):
    in_specs = (
        P("sp", None),
        P("sp", "tp"),
        P("sp", "tp"),
        P("sp", "tp"),
        P("sp", "tp"),
        P("tp", "sp"),
        P("tp", "sp"),
        P("tp"),
        P(),
        P("tp", None),
        P(),
        P(),
        P("sp", None),
        P("sp", None),
        P("sp", None, "tp"),
        P("sp", None, "tp"),
        P("sp", "tp", None),
    )
    out_specs = P("sp", None)
    return jax.shard_map(
        any_size, mesh=mesh, in_specs=in_specs, out_specs=out_specs, check_vma=False
    )
```

profile of v0, /device:TPU:25, one launch (start us, length us, event | category | flops | bytes accessed | tf_op | source)
XLA Modules:
  0.0 83.3 jit_solution(6934061135971895691)
XLA Ops:
  0.0 81.4 %shard_map.163 = bf16[128,2048]{1,0:T(8,128)(2,1)} custom-call(bf16[128,2048]{1,0:T(8,128)(2,1)} %residual_ref.1, bf16[128,512]{1,0:T(8,128)(2,1)} %query_ref.1, bf16[128,512]{1,0:T(8,128)(2,1)} %key_ref.1, bf16[128,512]{1,0:T(8,128)(2,1)} %value_ref.1, bf16[128,512]{1,0:T(8,128)(2,1)} %out_gate_ref.1, bf16[4,128]{1,0:T(4,128)(2,1)} %beta_ref.1, ...), custom_call_target="tpu_custom_call" | custom-call | tf_op jit(solution)/shard_map/pallas_call | solution.py:755
  81.4 1.9 %copy.19 = bf16[128,2048]{1,0:T(8,128)(2,1)} copy(bf16[128,2048]{1,0:T(8,128)(2,1)} %shard_map.163) | data formatting | bytes 1048576
where the time goes:
time: 83.5 us; the launch traced here: 83.3 us
  Pallas kernels  81.4 us (97%)
  local copies, waits for them, and re-layouts  1.88 us (2%)
    pallas_call x1, Pallas kernels, fused(): pl.pallas_call(functools.partial(layer_kernel, n_sp, n_tp), out_shape=jax...  81.4 us
    unnamed x1, local copies, waits for them, and re-layouts  1.88 us

commit v1 on v0

--- a/solution.py
+++ b/solution.py
@@ -754,7 +754,7 @@
     dma = pltpu.SemaphoreType.DMA
     return pl.pallas_call(
         functools.partial(layer_kernel, n_sp, n_tp),
-        out_shape=jax.ShapeDtypeStruct((length, width), low),
+        out_shape=pltpu.VMEM((length, width), low),
         in_specs=[vmem] * 13 + [hbm] * 4,
         out_specs=vmem,
         scratch_shapes=[

time: 83.5 us -> 81.6 us (0.977)
  local copies, waits for them, and re-layouts: 1.88 us -> 0.8 us
    unnamed x1, local copies, waits for them, and re-layouts: 1.88 us -> 0.8 us
where the time goes in v1:
time: 81.6 us; the launch traced here: 81.5 us
  Pallas kernels  80.7 us (99%)
    pallas_call x1, Pallas kernels, fused(): pl.pallas_call(functools.partial(layer_kernel, n_sp, n_tp), out_shape=plt...  80.7 us

profile of v1, /device:TPU:25, one launch (start us, length us, event | category | flops | bytes accessed | tf_op | source)
XLA Modules:
  0.0 81.5 jit_solution(96156070996205892)
XLA Ops:
  0.0 80.7 %shard_map.163 = bf16[128,2048]{1,0:T(8,128)(2,1)S(1)} custom-call(bf16[128,2048]{1,0:T(8,128)(2,1)} %residual_ref.1, bf16[128,512]{1,0:T(8,128)(2,1)} %query_ref.1, bf16[128,512]{1,0:T(8,128)(2,1)} %key_ref.1, bf16[128,512]{1,0:T(8,128)(2,1)} %value_ref.1, bf16[128,512]{1,0:T(8,128)(2,1)} %out_gate_ref.1, bf16[4,128]{1,0:T(4,128)(2,1)} %beta_ref.1, ...), custom_call_target="tpu_custom_call" | custom-call | tf_op jit(solution)/shard_map/pallas_call | solution.py:755
  80.7 0.8 copy.19

commit v2 on v1

--- a/solution.py
+++ b/solution.py
@@ -13,6 +13,8 @@
 TOP = 2
 BLOCK = 64
 GROUP = 2
+VISITS = ((1, 0, 3, 2), (0, 2, 3, 1), (0, 1, 3, 2), (2, 1, 0, 3))
+FAR = ((1, 3, 2), (0, 2, 3), (0, 1, 3), (2, 1, 0))
 
 
 highest_precision = lax.Precision.HIGHEST
@@ -267,6 +269,23 @@
     )
 
 
+scope = jax.named_scope
+
+
+def pick(table, home):
+    chosen = []
+    for i in range(len(table[0])):
+        value = 0
+        for h, order in enumerate(table):
+            value = value + (home == h).astype(jnp.int32) * order[i]
+        chosen.append(value)
+    return chosen
+
+
+def drain(ref, sem):
+    pltpu.make_async_copy(ref, ref, sem).wait()
+
+
 def layer_kernel(
     n_sp,
     n_tp,
@@ -296,6 +315,9 @@
     adds_v,
     state_in,
     state_out,
+    mate_out,
+    mate_in,
+    entry_v,
     mixed_v,
     readout_v,
     gated_v,
@@ -310,11 +332,17 @@
     pair_v,
     result_v,
     back_v,
+    final_v,
     local_sem,
+    sent_sem,
     state_sem,
+    mate_sem,
+    entry_sem,
     proj_sem,
-    send_sem,
-    fan_sem,
+    arrive_sem,
+    near_sem,
+    full_sem,
+    pair_sem,
     part_sem,
     back_sem,
     out_sem,
@@ -331,6 +359,8 @@
     feat = HEAD_FEATURES
     hidden_units = gate_v.shape[1]
 
+    with scope("a_start"):
+        pass
     local = [
         pltpu.make_async_copy(out_weight_hbm, out_weight_v, local_sem.at[0]),
         pltpu.make_async_copy(gate_hbm.at[0], gate_v, local_sem.at[1]),
@@ -416,42 +446,95 @@
         inverses = [inv - mm(inv, step) for inv, step in zip(inverses, steps)]
         size *= 2
     solved = [mm(inv, right).astype(jnp.bfloat16) for inv, right in zip(inverses, rights)]
+    home, core = s // group, s % group
+    mate = home * group + (1 - core)
+    after = lax.rem(s + group, n_sp)
+
+    def mate_copy(h):
+        return remote(
+            mate_out.at[h], mate_in.at[h], sent_sem.at[0], mate_sem.at[h], mate, t
+        )
+
+    def state_copy(h):
+        return remote(
+            state_out.at[h], state_in.at[h], sent_sem.at[1], state_sem.at[h], after, t
+        )
+
+    def entry_copy(h):
+        return remote(
+            state_in.at[h], entry_v.at[h], sent_sem.at[2], entry_sem.at[h], mate, t
+        )
+
     for h in range(heads):
         ends = mm_tn(kd_list[h], solved[h])
         adds_v[h] = ends[:, :feat]
-        maps_v[h] = (last_list[h] * eye[:feat, :feat] - ends[:, feat:]).astype(jnp.bfloat16)
+        maps = (last_list[h] * eye[:feat, :feat] - ends[:, feat:]).astype(jnp.bfloat16)
+        maps_v[h] = maps
+        mate_out[h, 0] = maps
+        mate_out[h, 1] = ends[:, :feat].astype(jnp.bfloat16)
+
+    with scope("b_barrier"):
+        pl.semaphore_wait(barrier, n_sp - 1 + n_tp - 1)
+
+    @pl.when(core == 0)
+    def _():
+        for h in range(heads):
+            mate_copy(h).start()
+
     for h in range(heads):
         seen = mm(score_list[h], solved[h])
         mixed_v[h] = seen[:, :feat]
         readout_v[h] = (q_list[h] - seen[:, feat:]).astype(jnp.bfloat16)
 
-    pl.semaphore_wait(barrier, n_sp - 1 + n_tp - 1)
-
-    after = lax.rem(s + 1, n_sp)
-
-    def state_copy(h):
-        return remote(
-            state_out.at[h], state_in.at[h], state_sem.at[0, h], state_sem.at[1, h], after, t
-        )
-
-    @pl.when(s == 0)
-    def _():
-        state_in[...] = jnp.zeros_like(state_in)
-
-    for h in range(heads):
-
-        @pl.when(s > 0)
+    @pl.when(core == 1)
+    def _():
+        for h in range(heads):
+            with scope("c_mate"):
+                mate_copy(h).wait_recv()
+
+            @pl.when(home == 0)
+            def _():
+                state_out[h] = (mm(maps_v[h], mate_in[h, 1]) + adds_v[h]).astype(jnp.bfloat16)
+                state_copy(h).start()
+                entry_v[h] = mate_in[h, 1]
+
+            @pl.when(home > 0)
+            def _():
+                both = mm(maps_v[h], jnp.concatenate([mate_in[h, 0], mate_in[h, 1]], 1))
+                maps_v[h] = both[:, :feat].astype(jnp.bfloat16)
+                adds_v[h] = adds_v[h] + both[:, feat:]
+
+        @pl.when(home > 0)
         def _():
-            state_copy(h).wait_recv()
-
-        @pl.when(s < n_sp - 1)
-        def _():
-            state_out[h] = (mm(maps_v[h], state_in[h]) + adds_v[h]).astype(jnp.bfloat16)
-            state_copy(h).start()
+            for h in range(heads):
+                with scope("c_state"):
+                    state_copy(h).wait_recv()
+
+                @pl.when(home < chunks - 1)
+                def _():
+                    state_out[h] = (mm(maps_v[h], state_in[h]) + adds_v[h]).astype(jnp.bfloat16)
+                    state_copy(h).start()
+
+                entry_copy(h).start()
+
+            for h in range(heads):
+                entry_v[h] = (
+                    mm(mate_in[h, 0], state_in[h]) + mate_in[h, 1].astype(jnp.float32)
+                ).astype(jnp.bfloat16)
+
+    @pl.when((core == 0) & (home == 0))
+    def _():
+        entry_v[...] = jnp.zeros_like(entry_v)
+
+    @pl.when((core == 0) & (home > 0))
+    def _():
+        for h in range(heads):
+            with scope("c_state"):
+                entry_copy(h).wait_recv()
 
     for h in range(heads):
         cols = slice(h * feat, (h + 1) * feat)
-        mixed = mixed_v[h] + mm(readout_v[h], state_in[h])
+        mixed = mixed_v[h] + mm(readout_v[h], entry_v[h])
         normalized = (
             mixed * lax.rsqrt(jnp.mean(mixed * mixed, -1, keepdims=True) + 1e-06) * head_gain_ref[...]
         )
@@ -459,6 +542,9 @@
         gated_v[:, cols] = (normalized * (gate * jax.nn.sigmoid(gate))).astype(jnp.bfloat16)
 
     local[0].wait()
+
+    def row_block(i):
+        return pl.ds(pl.multiple_of(i * rows, rows), rows)
 
     def project(i, carry):
         cols = pl.ds(pl.multiple_of(i * 512, 512), 512)
@@ -467,19 +553,21 @@
         ).astype(jnp.bfloat16)
         return carry
 
-    lax.fori_loop(0, width // 512, project, 0)
-
-    def row_block(i):
-        return pl.ds(pl.multiple_of(i * rows, rows), rows)
-
-    proj_copies = []
-    for k in range(1, n_tp):
-        to = lax.rem(t + k, n_tp)
-        copy = remote(
-            proj_v.at[row_block(to)], proj_in.at[k - 1], proj_sem.at[0, k - 1], proj_sem.at[1, k - 1], s, to
-        )
-        copy.start()
-        proj_copies.append(copy)
+    for part, cols in enumerate((left, right)):
+        steps = half // 512
+        with scope("d_project"):
+            lax.fori_loop(part * steps, (part + 1) * steps, project, 0)
+        for k in range(1, n_tp):
+            to = lax.rem(t + k, n_tp)
+            copy = remote(
+                proj_v.at[row_block(to), cols],
+                proj_in.at[k - 1, :, cols],
+                sent_sem.at[3],
+                proj_sem.at[0],
+                s,
+                to,
+            )
+            copy.start()
 
     own_row = (
         lax.broadcasted_iota(jnp.int32, (rows, length), 1)
@@ -506,63 +594,43 @@
 
     def send_copy(to):
         return remote(
-            send_v.at[to],
-            arrived_v.at[s // group, t, s % group],
-            send_sem.at[0, to],
-            send_sem.at[1, s],
-            to,
-            t,
-        )
-
-    def arrival(p):
-        return remote(
-            send_v.at[p],
-            arrived_v.at[p // group, t, p % group],
-            send_sem.at[0, p],
-            send_sem.at[1, p],
-            p,
-            t,
-        )
-
-    def fan_copies(c):
-        mine = arrived_v.at[c, t]
-        return [
-            remote(mine, mine, fan_sem.at[0, 0, c], fan_sem.at[0, 1, c], s, tx),
-            remote(mine, mine, fan_sem.at[1, 0, c], fan_sem.at[1, 1, c], s, ty),
-        ]
-
-    def relay_copies(c):
-        a = arrived_v.at[c, tx, :, :, left]
-        b = arrived_v.at[c, ty, :, :, right]
-        return [
-            remote(a, a, fan_sem.at[2, 0, c], fan_sem.at[2, 1, c], s, ty),
-            remote(b, b, fan_sem.at[3, 0, c], fan_sem.at[3, 1, c], s, tx),
-        ]
-
-    def fan_out(c):
-        for p in range(c * group, (c + 1) * group):
-
-            @pl.when(s != p)
-            def _():
-                arrival(p).wait_recv()
-
-        for copy in fan_copies(c):
-            copy.start()
-
-    def relay(c):
-        for copy, onward in zip(fan_copies(c), relay_copies(c)):
-            copy.wait_recv()
-            onward.start()
-
-    home = s // group
-
-    @pl.when(home >= 2)
-    def _():
-        fan_out(0)
+            send_v.at[to], arrived_v.at[home, t, core], sent_sem.at[4], arrive_sem.at[home], to, t
+        )
+
+    order = pick(VISITS, home)
+    legs = [(home, core, 1), (home, 1 - core, 1)] + [(c, 0, group) for c in pick(FAR, home)]
+
+    def fan_out(j):
+        c, low, count = legs[j]
+        if j > 0:
+            with scope("g_arrive"):
+                drain(arrived_v.at[c, t, pl.ds(low, count)], arrive_sem.at[c])
+
+        def one(cols, sem, to):
+            mine = arrived_v.at[c, t, pl.ds(low, count), :, cols]
+            remote(mine, mine, sent_sem.at[5], sem, s, to).start()
+
+        one(left, near_sem.at[j, 0], tx)
+        one(right, near_sem.at[j, 1], ty)
+        one(right, full_sem.at[c], tx)
+        one(left, full_sem.at[c], ty)
+
+    def relay(j):
+        c, low, count = legs[j]
+        for i, (near, cols, to) in enumerate(((tx, left, ty), (ty, right, tx))):
+            block = arrived_v.at[c, near, pl.ds(low, count), :, cols]
+            with scope("h_fan"):
+                drain(block, near_sem.at[j, i])
+            remote(block, block, sent_sem.at[5], full_sem.at[c], s, to).start()
+
+    def wait_full(k):
+        with scope("j_full"):
+            drain(arrived_v.at[order[k], pl.ds(0, 2)], full_sem.at[order[k]])
 
     projected = proj_v[row_block(t), :].astype(jnp.float32)
+    with scope("e_proj"):
+        drain(proj_in, proj_sem.at[0])
     for k in range(1, n_tp):
-        proj_copies[k - 1].wait_recv()
         projected = projected + proj_in[k - 1].astype(jnp.float32)
     residual = residual_ref[row_block(t), :].astype(jnp.float32)
     hidden_in = layer_norm(residual_scale * residual + projected, norm_gain_ref[...]).astype(
@@ -572,27 +640,37 @@
 
     send_v[...] = mm_tn(table, hidden_in).astype(jnp.bfloat16).reshape(n_sp, cap, width)
 
-    for k in range(1, n_sp):
-        send_copy(lax.rem(s + k, n_sp)).start()
-    arrived_v[home, t, s % group] = send_v[s]
-
-    def part_copies(c):
-        def one(kind, src, to):
-            return remote(
-                src, part_in.at[kind, c], part_sem.at[kind, 0, c], part_sem.at[kind, 1, c], s, to
-            )
-
-        return [
-            one(0, part_v.at[c, td, :, left], tx),
-            one(1, part_v.at[c, td, :, right], ty),
-            one(2, part_v.at[c, tx, :, left], tx),
-            one(3, part_v.at[c, ty, :, right], ty),
-            one(4, pair_v.at[0, c], ty),
-            one(5, pair_v.at[1, c], tx),
-        ]
-
-    def gate_up(c):
-        piece = arrived_v[c].reshape(n_tp * group * cap, width)
+    for i in range(group):
+
+        @pl.when(s != home * group + i)
+        def _():
+            send_copy(home * group + i).start()
+
+    for far in range(1, chunks):
+        for there in (home - far, home + far):
+
+            @pl.when((there >= 0) & (there < chunks))
+            def _():
+                for i in range(group):
+                    send_copy(there * group + i).start()
+
+    arrived_v[home, t, core] = send_v[s]
+
+    def part_copy(kind, j):
+        src, to = (
+            (part_v.at[j, td, :, left], tx),
+            (part_v.at[j, td, :, right], ty),
+            (part_v.at[j, tx, :, left], tx),
+            (part_v.at[j, ty, :, right], ty),
+            (pair_v.at[0, j], ty),
+            (pair_v.at[1, j], tx),
+        )[kind]
+        sem = pair_sem.at[j, kind] if kind < 2 else part_sem.at[j]
+        return remote(src, part_in.at[kind, j], sent_sem.at[6], sem, s, to)
+
+    def gate_up(j, part):
+        piece = arrived_v[order[j]].reshape(n_tp * group * cap, width)
+        steps = hidden_units // 256 // 2
 
         def step(i, carry):
             cols = pl.ds(pl.multiple_of(i * 256, 256), 256)
@@ -601,141 +679,186 @@
             inner_v[:, cols] = (gate * jax.nn.sigmoid(gate) * up).astype(jnp.bfloat16)
             return carry
 
-        lax.fori_loop(0, hidden_units // 256, step, 0)
-
-    def down(c):
+        with scope("k_gateup"):
+            lax.fori_loop(part * steps, (part + 1) * steps, step, 0)
+
+    def down(j):
         def step(i, carry):
             cols = pl.ds(pl.multiple_of(i * 512, 512), 512)
-            part_v[c, :, :, cols] = (
-                jnp.dot(inner_v[...], down_v[:, cols], preferred_element_type=jnp.float32)
+            part_v[j, :, :, cols] = (
+                jnp.dot(
+                    inner_v[...], down_v[:, cols], preferred_element_type=jnp.float32
+                )
                 .astype(jnp.bfloat16)
                 .reshape(n_tp, group * cap, 512)
             )
             return carry
 
-        lax.fori_loop(0, width // 512, step, 0)
-
-    def pair_up(c):
-        copies = part_copies(c)
+        steps = half // 512
+        for part in range(2):
+            with scope("l_down"):
+                lax.fori_loop(part * steps, (part + 1) * steps, step, 0)
+            part_copy(part, j).start()
+            part_copy(2 + part, j).start()
+
+    def pair_up(j):
         wide = jnp.float32
-        copies[0].wait_recv()
-        pair_v[0, c] = (part_v[c, ty, :, left].astype(wide) + part_in[0, c].astype(wide)).astype(
-            jnp.bfloat16
-        )
-        copies[4].start()
-        copies[1].wait_recv()
-        pair_v[1, c] = (part_v[c, tx, :, right].astype(wide) + part_in[1, c].astype(wide)).astype(
-            jnp.bfloat16
-        )
-        copies[5].start()
-
-    def back_copy(c, i):
-        return remote(
-            result_v.at[c, i],
-            back_v.at[s],
-            back_sem.at[0, c * group + i],
-            back_sem.at[1, s],
-            c * group + i,
-            t,
-        )
-
-    def finish(c):
-        copies = part_copies(c)
-        for i in range(2, 6):
-            copies[i].wait_recv()
-        own = part_v[c, t].astype(jnp.float32)
-        near, far = part_in[2, c].astype(jnp.float32), part_in[4, c].astype(jnp.float32)
-        low = own[:, left] + near + far
-        near, far = part_in[3, c].astype(jnp.float32), part_in[5, c].astype(jnp.float32)
-        high = own[:, right] + near + far
-        result_v[c, :, :, left] = low.astype(jnp.bfloat16).reshape(group, cap, half)
-        result_v[c, :, :, right] = high.astype(jnp.bfloat16).reshape(group, cap, half)
+        for i, (near, cols) in enumerate(((ty, left), (tx, right))):
+            with scope("m_pair"):
+                drain(part_in.at[i, j], pair_sem.at[j, i])
+            pair_v[i, j] = (
+                part_v[j, near, :, cols].astype(wide) + part_in[i, j].astype(wide)
+            ).astype(jnp.bfloat16)
+            part_copy(4 + i, j).start()
+
+    def finish(j):
+        with scope("n_finish"):
+            drain(part_in.at[pl.ds(2, 4), j], part_sem.at[j])
+        for i, cols in enumerate((left, right)):
+            near = part_in[2 + i, j].astype(jnp.float32)
+            far = part_in[4 + i, j].astype(jnp.float32)
+            total = part_v[j, t, :, cols].astype(jnp.float32) + near + far
+            result_v[j, :, :, cols] = total.astype(jnp.bfloat16).reshape(group, cap, half)
         for i in range(group):
-            p = c * group + i
+            p = order[j] * group + i
 
             @pl.when(s != p)
             def _():
-                back_copy(c, i).start()
+                remote(
+                    result_v.at[j, i], back_v.at[s], sent_sem.at[7], back_sem.at[0], p, t
+                ).start()
 
             @pl.when(s == p)
             def _():
-                back_v[p] = result_v[c, i]
-
-    @pl.when(home < 2)
-    def _():
-        fan_out(0)
-
-    relay(0)
-    if chunks > 1:
-        fan_out(1)
-    for copy in local[1:]:
+                back_v[s] = result_v[j, i]
+
+    fan_out(0)
+    fan_out(1)
+
+    @pl.when(home == 0)
+    def _():
+        relay(0)
+        relay(1)
+
+    fan_out(2)
+
+    @pl.when(home > 0)
+    def _():
+        relay(0)
+        relay(1)
+
+    for copy in local[1:4]:
         copy.wait()
-    for i in range(chunks + 2):
-        if i < chunks:
-            for copy in relay_copies(i):
-                copy.wait_recv()
-            gate_up(i)
-            if i + 1 < chunks:
-                relay(i + 1)
-            if i + 2 < chunks:
-                fan_out(i + 2)
-            down(i)
-            for copy in part_copies(i)[:4]:
-                copy.start()
-        if 1 <= i <= chunks:
-            pair_up(i - 1)
-        if i >= 2:
-            finish(i - 2)
-
-    for p in range(n_sp):
-
-        @pl.when(s != p)
-        def _():
-            remote(
-                result_v.at[0, 0], back_v.at[p], back_sem.at[0, p], back_sem.at[1, p], p, t
-            ).wait_recv()
+    relay(2)
+
+    @pl.when(home > 0)
+    def _():
+        fan_out(3)
+
+    wait_full(0)
+    gate_up(0, 0)
+
+    @pl.when(home > 0)
+    def _():
+        relay(3)
+        fan_out(4)
+
+    gate_up(0, 1)
+
+    @pl.when(home == 0)
+    def _():
+        fan_out(3)
+
+    down(0)
+    wait_full(1)
+    gate_up(1, 0)
+
+    @pl.when(home > 0)
+    def _():
+        relay(4)
+
+    gate_up(1, 1)
+
+    @pl.when(home == 0)
+    def _():
+        relay(3)
+        fan_out(4)
+
+    pair_up(0)
+    down(1)
+    wait_full(2)
+    gate_up(2, 0)
+
+    @pl.when(home == 0)
+    def _():
+        relay(4)
+
+    gate_up(2, 1)
+    pair_up(1)
+    finish(0)
+    down(2)
+    wait_full(3)
+    gate_up(3, 0)
+    gate_up(3, 1)
+    pair_up(2)
+    finish(1)
+    down(3)
+    finish(2)
+    pair_up(3)
+    finish(3)
+
+    with scope("o_back"):
+        drain(back_v.at[pl.ds(0, n_sp - 1)], back_sem.at[0])
 
     back = back_v[...].reshape(slots, width)
     routed = jnp.zeros((rows, width), jnp.float32)
     for j in range(TOP):
         routed = routed + weights[:, j : j + 1] * mm(tables[j], back)
-    out_ref[row_block(t), :] = layer_norm(
+    final_v[...] = layer_norm(
         residual_scale * hidden_v[...].astype(jnp.float32) + routed, final_gain_ref[...]
     ).astype(jnp.bfloat16)
 
-    out_copies = []
-    for k in range(1, n_tp):
-        copy = remote(
-            out_ref.at[row_block(t)],
-            out_ref.at[row_block(t)],
-            out_sem.at[0, k - 1],
-            out_sem.at[1, k - 1],
-            s,
-            lax.rem(t + k, n_tp),
-        )
-        copy.start()
-        out_copies.append(copy)
-
-    @pl.when(s < n_sp - 1)
-    def _():
-        for h in range(heads):
-            state_copy(h).wait_send()
-
-    for copy in proj_copies:
-        copy.wait_send()
-    for k in range(1, n_sp):
-        send_copy(lax.rem(s + k, n_sp)).wait_send()
-    for c in range(chunks):
-        for copy in fan_copies(c) + relay_copies(c) + part_copies(c):
-            copy.wait_send()
-        for i in range(group):
-
-            @pl.when(s != c * group + i)
-            def _():
-                back_copy(c, i).wait_send()
-
-    for copy in out_copies:
-        copy.wait()
+    def out_copy(owner, q, to, sem):
+        cols = pl.ds(q * (width // 4), width // 4)
+        cells = out_ref.at[row_block(owner), cols]
+        source = final_v.at[:, cols] if owner is t else cells
+        return remote(source, cells, sent_sem.at[8], out_sem.at[sem], s, to)
+
+    for q in range(4):
+        out_copy(t, q, tx, min(q, 2)).start()
+        out_copy(t, 3 - q, ty, min(q, 2) + (3 if q < 2 else 0)).start()
+    own_copy = pltpu.make_async_copy(final_v, out_ref.at[row_block(t)], local_sem.at[4])
+    own_copy.start()
+    piece = final_v.at[:, pl.ds(0, width // 4)]
+    with scope("q_out"):
+        for q in range(2):
+            drain(piece, out_sem.at[q])
+            out_copy(tx, q, ty, 2).start()
+            drain(piece, out_sem.at[3 + q])
+            out_copy(ty, 3 - q, tx, 2).start()
+
+    @pl.when(core == 0)
+    def _():
+        drain(mate_out, sent_sem.at[0])
+
+    @pl.when((core == 1) & (home < chunks - 1))
+    def _():
+        drain(state_out, sent_sem.at[1])
+
+    @pl.when((core == 1) & (home > 0))
+    def _():
+        drain(state_in, sent_sem.at[2])
+
+    drain(proj_in, sent_sem.at[3])
+    drain(send_v.at[pl.ds(0, n_sp - 1)], sent_sem.at[4])
+    drain(arrived_v.at[:, pl.ds(0, 3)], sent_sem.at[5])
+    drain(part_in, sent_sem.at[6])
+    drain(back_v.at[pl.ds(0, n_sp - 1)], sent_sem.at[7])
+    own_copy.wait()
+    with scope("r_out"):
+        drain(proj_in.at[pl.ds(0, 2)], out_sem.at[2])
+    with scope("s_sends"):
+        drain(proj_in, sent_sem.at[8])
 
 
 def fused(args, n_sp, n_tp, cap):
@@ -756,7 +879,7 @@
         functools.partial(layer_kernel, n_sp, n_tp),
         out_shape=pltpu.VMEM((length, width), low),
         in_specs=[vmem] * 13 + [hbm] * 4,
-        out_specs=vmem,
+        out_specs=hbm,
         scratch_shapes=[
             pltpu.VMEM(out_weight.shape, low),
             pltpu.VMEM(expert_gate.shape[1:], low),
@@ -765,6 +888,9 @@
             pltpu.VMEM((heads, feat, feat), low),
             pltpu.VMEM((heads, feat, feat), full),
             pltpu.VMEM((heads, feat, feat), low),
+            pltpu.VMEM((heads, feat, feat), low),
+            pltpu.VMEM((heads, 2, feat, feat), low),
+            pltpu.VMEM((heads, 2, feat, feat), low),
             pltpu.VMEM((heads, feat, feat), low),
             pltpu.VMEM((heads, length, feat), full),
             pltpu.VMEM((heads, length, feat), low),
@@ -780,14 +906,20 @@
             pltpu.VMEM((2, chunks, GROUP * cap, width // 2), low),
             pltpu.VMEM((chunks, GROUP, cap, width), low),
             pltpu.VMEM((n_sp, cap, width), low),
-            dma((4,)),
-            dma((2, heads)),
-            dma((2, n_tp - 1)),
-            dma((2, n_sp)),
-            dma((4, 2, chunks)),
-            dma((6, 2, chunks)),
-            dma((2, n_sp)),
-            dma((2, n_tp - 1)),
+            pltpu.VMEM((rows, width), low),
+            dma((5,)),
+            dma((9,)),
+            dma((heads,)),
+            dma((heads,)),
+            dma((heads,)),
+            dma((1,)),
+            dma((chunks,)),
+            dma((chunks + 1, 2)),
+            dma((chunks,)),
+            dma((chunks, 2)),
+            dma((chunks,)),
+            dma((1,)),
+            dma((5,)),
         ],
         compiler_params=pltpu.CompilerParams(
             collective_id=0, has_side_effects=True, vmem_limit_bytes=60 * 1024 * 1024
@@ -808,8 +940,7 @@
     cap = 2 * TOP * (length // n_tp) // experts
     fits = (
         expert_gate.shape[0] == 1
-        and n_sp > GROUP
-        and n_sp % GROUP == 0
+        and n_sp == GROUP * len(VISITS)
         and n_tp == 4
         and length == HEAD_FEATURES
         and cap % 16 == 0

time: 81.6 us -> 74.4 us (0.912)
  the two profiles are of different devices: /device:TPU:25 before, /device:TPU:16 now
where the time goes in v2:
time: 74.4 us; the launch traced here: 74.3 us
  Pallas kernels  73.5 us (99%)
  local copies, waits for them, and re-layouts  0.8 us (1%)
    pallas_call x1, Pallas kernels, fused(): pl.pallas_call(functools.partial(layer_kernel, n_sp, n_tp), out_shape=plt...  73.5 us

profile of v2, /device:TPU:16, one launch (start us, length us, event | category | flops | bytes accessed | tf_op | source)
XLA Modules:
  0.0 74.3 jit_solution(1737340727774375953)
XLA Ops:
  0.0 73.5 %shard_map.163 = bf16[128,2048]{1,0:T(8,128)(2,1)S(1)} custom-call(bf16[128,2048]{1,0:T(8,128)(2,1)} %residual_ref.1, bf16[128,512]{1,0:T(8,128)(2,1)} %query_ref.1, bf16[128,512]{1,0:T(8,128)(2,1)} %key_ref.1, bf16[128,512]{1,0:T(8,128)(2,1)} %value_ref.1, bf16[128,512]{1,0:T(8,128)(2,1)} %out_gate_ref.1, bf16[4,128]{1,0:T(4,128)(2,1)} %beta_ref.1, ...), custom_call_target="tpu_custom_call" | custom-call | tf_op jit(solution)/shard_map/pallas_call | solution.py:878
  73.5 0.8 %copy.19 = bf16[128,2048]{1,0:T(8,128)(2,1)} copy(bf16[128,2048]{1,0:T(8,128)(2,1)S(1)} %shard_map.163) | data formatting | bytes 1048576

commit v3 on v2

--- a/solution.py
+++ b/solution.py
@@ -13,8 +13,8 @@
 TOP = 2
 BLOCK = 64
 GROUP = 2
-VISITS = ((1, 0, 3, 2), (0, 2, 3, 1), (0, 1, 3, 2), (2, 1, 0, 3))
-FAR = ((1, 3, 2), (0, 2, 3), (0, 1, 3), (2, 1, 0))
+VISITS = ((1, 2, 3, 0), (0, 2, 3, 1), (0, 3, 1, 2), (0, 1, 2, 3))
+SENDS = ((1, 2, 3), (0, 2, 3), (3, 0, 1), (2, 0, 1))
 
 
 highest_precision = lax.Precision.HIGHEST
@@ -289,6 +289,24 @@
 def layer_kernel(
     n_sp,
     n_tp,
+    residual_hbm,
+    query_hbm,
+    key_hbm,
+    value_hbm,
+    out_gate_hbm,
+    beta_hbm,
+    decay_hbm,
+    decay_log_hbm,
+    head_gain_hbm,
+    norm_gain_hbm,
+    final_gain_hbm,
+    index_hbm,
+    weights_hbm,
+    out_weight_hbm,
+    gate_hbm,
+    up_hbm,
+    down_hbm,
+    out_ref,
     residual_ref,
     query_ref,
     key_ref,
@@ -302,11 +320,6 @@
     final_gain_ref,
     index_ref,
     weights_ref,
-    out_weight_hbm,
-    gate_hbm,
-    up_hbm,
-    down_hbm,
-    out_ref,
     out_weight_v,
     gate_v,
     up_v,
@@ -327,6 +340,7 @@
     send_v,
     arrived_v,
     inner_v,
+    own_inner_v,
     part_v,
     part_in,
     pair_v,
@@ -359,17 +373,6 @@
     feat = HEAD_FEATURES
     hidden_units = gate_v.shape[1]
 
-    with scope("a_start"):
-        pass
-    local = [
-        pltpu.make_async_copy(out_weight_hbm, out_weight_v, local_sem.at[0]),
-        pltpu.make_async_copy(gate_hbm.at[0], gate_v, local_sem.at[1]),
-        pltpu.make_async_copy(up_hbm.at[0], up_v, local_sem.at[2]),
-        pltpu.make_async_copy(down_hbm.at[0], down_v, local_sem.at[3]),
-    ]
-    for copy in local:
-        copy.start()
-
     barrier = pltpu.get_barrier_semaphore()
     for k in range(1, n_sp):
         pl.semaphore_signal(
@@ -379,6 +382,29 @@
         pl.semaphore_signal(
             barrier, inc=1, device_id=(s, lax.rem(t + k, n_tp)), device_id_type=MESH
         )
+
+    pairs = [
+        (decay_hbm, decay_ref),
+        (decay_log_hbm, decay_log_ref),
+        (beta_hbm, beta_ref),
+        (key_hbm, key_ref),
+        (query_hbm, query_ref),
+        (value_hbm, value_ref),
+        (out_gate_hbm, out_gate_ref),
+        (head_gain_hbm, head_gain_ref),
+        (out_weight_hbm, out_weight_v),
+        (index_hbm, index_ref),
+        (weights_hbm, weights_ref),
+        (residual_hbm, residual_ref),
+        (norm_gain_hbm, norm_gain_ref),
+        (final_gain_hbm, final_gain_ref),
+        (gate_hbm.at[0], gate_v),
+        (up_hbm.at[0], up_v),
+        (down_hbm.at[0], down_v),
+    ]
+    local = [pltpu.make_async_copy(a, b, local_sem.at[i]) for i, (a, b) in enumerate(pairs)]
+    for copy in local:
+        copy.start()
 
     def remote(src, dst, sem_a, sem_b, to_s, to_t):
         return pltpu.make_async_remote_copy(
@@ -390,6 +416,9 @@
             device_id_type=MESH,
         )
 
+    with scope("a_load"):
+        for copy in local[:6]:
+            copy.wait()
     row_id = lax.broadcasted_iota(jnp.int32, (length, length), 0)
     col_id = lax.broadcasted_iota(jnp.int32, (length, length), 1)
     causal = row_id >= col_id
@@ -532,6 +561,8 @@
             with scope("c_state"):
                 entry_copy(h).wait_recv()
 
+    local[6].wait()
+    local[7].wait()
     for h in range(heads):
         cols = slice(h * feat, (h + 1) * feat)
         mixed = mixed_v[h] + mm(readout_v[h], entry_v[h])
@@ -541,7 +572,7 @@
         gate = out_gate_ref[:, cols].astype(jnp.float32)
         gated_v[:, cols] = (normalized * (gate * jax.nn.sigmoid(gate))).astype(jnp.bfloat16)
 
-    local[0].wait()
+    local[8].wait()
 
     def row_block(i):
         return pl.ds(pl.multiple_of(i * rows, rows), rows)
@@ -569,6 +600,8 @@
             )
             copy.start()
 
+    for copy in local[9:14]:
+        copy.wait()
     own_row = (
         lax.broadcasted_iota(jnp.int32, (rows, length), 1)
         == lax.broadcasted_iota(jnp.int32, (rows, length), 0) + t * rows
@@ -598,7 +631,7 @@
         )
 
     order = pick(VISITS, home)
-    legs = [(home, core, 1), (home, 1 - core, 1)] + [(c, 0, group) for c in pick(FAR, home)]
+    legs = [(home, core, 1), (home, 1 - core, 1)] + [(c, 0, group) for c in order[:-1]]
 
     def fan_out(j):
         c, low, count = legs[j]
@@ -646,13 +679,9 @@
         def _():
             send_copy(home * group + i).start()
 
-    for far in range(1, chunks):
-        for there in (home - far, home + far):
-
-            @pl.when((there >= 0) & (there < chunks))
-            def _():
-                for i in range(group):
-                    send_copy(there * group + i).start()
+    for there in pick(SENDS, home):
+        for i in range(group):
+            send_copy(there * group + i).start()
 
     arrived_v[home, t, core] = send_v[s]
 
@@ -665,10 +694,10 @@
             (pair_v.at[0, j], ty),
             (pair_v.at[1, j], tx),
         )[kind]
-        sem = pair_sem.at[j, kind] if kind < 2 else part_sem.at[j]
+        sem = pair_sem.at[j, kind] if kind < 2 else part_sem.at[j, kind % 2]
         return remote(src, part_in.at[kind, j], sent_sem.at[6], sem, s, to)
 
-    def gate_up(j, part):
+    def gate_up(j, part, inner):
         piece = arrived_v[order[j]].reshape(n_tp * group * cap, width)
         steps = hidden_units // 256 // 2
 
@@ -676,18 +705,18 @@
             cols = pl.ds(pl.multiple_of(i * 256, 256), 256)
             gate = jnp.dot(piece, gate_v[:, cols], preferred_element_type=jnp.float32)
             up = jnp.dot(piece, up_v[:, cols], preferred_element_type=jnp.float32)
-            inner_v[:, cols] = (gate * jax.nn.sigmoid(gate) * up).astype(jnp.bfloat16)
+            inner[:, cols] = (gate * jax.nn.sigmoid(gate) * up).astype(jnp.bfloat16)
             return carry
 
         with scope("k_gateup"):
             lax.fori_loop(part * steps, (part + 1) * steps, step, 0)
 
-    def down(j):
+    def down(j, inner, kinds):
         def step(i, carry):
             cols = pl.ds(pl.multiple_of(i * 512, 512), 512)
             part_v[j, :, :, cols] = (
                 jnp.dot(
-                    inner_v[...], down_v[:, cols], preferred_element_type=jnp.float32
+                    inner[...], down_v[:, cols], preferred_element_type=jnp.float32
                 )
                 .astype(jnp.bfloat16)
                 .reshape(n_tp, group * cap, 512)
@@ -698,8 +727,8 @@
         for part in range(2):
             with scope("l_down"):
                 lax.fori_loop(part * steps, (part + 1) * steps, step, 0)
-            part_copy(part, j).start()
-            part_copy(2 + part, j).start()
+            for kind in range(part, kinds, 2):
+                part_copy(kind, j).start()
 
     def pair_up(j):
         wide = jnp.float32
@@ -712,25 +741,30 @@
             part_copy(4 + i, j).start()
 
     def finish(j):
-        with scope("n_finish"):
-            drain(part_in.at[pl.ds(2, 4), j], part_sem.at[j])
         for i, cols in enumerate((left, right)):
+            with scope("n_finish"):
+                drain(part_in.at[pl.ds(0, 2), j], part_sem.at[j, i])
             near = part_in[2 + i, j].astype(jnp.float32)
             far = part_in[4 + i, j].astype(jnp.float32)
             total = part_v[j, t, :, cols].astype(jnp.float32) + near + far
             result_v[j, :, :, cols] = total.astype(jnp.bfloat16).reshape(group, cap, half)
-        for i in range(group):
-            p = order[j] * group + i
-
-            @pl.when(s != p)
-            def _():
-                remote(
-                    result_v.at[j, i], back_v.at[s], sent_sem.at[7], back_sem.at[0], p, t
-                ).start()
-
-            @pl.when(s == p)
-            def _():
-                back_v[s] = result_v[j, i]
+            for m in range(group):
+                p = order[j] * group + m
+
+                @pl.when(s != p)
+                def _():
+                    remote(
+                        result_v.at[j, m, :, cols],
+                        back_v.at[s, :, cols],
+                        sent_sem.at[7],
+                        back_sem.at[0],
+                        p,
+                        t,
+                    ).start()
+
+                @pl.when(s == p)
+                def _():
+                    back_v[s, :, cols] = result_v[j, m, :, cols]
 
     fan_out(0)
     fan_out(1)
@@ -747,65 +781,78 @@
         relay(0)
         relay(1)
 
-    for copy in local[1:4]:
+    for copy in local[14:]:
         copy.wait()
     relay(2)
 
-    @pl.when(home > 0)
+    @pl.when(home != 1)
     def _():
         fan_out(3)
 
+    own = chunks - 1
+
+    @pl.when(home != 1)
+    def _():
+        wait_full(own)
+        gate_up(own, 0, own_inner_v)
+
     wait_full(0)
-    gate_up(0, 0)
-
-    @pl.when(home > 0)
+    gate_up(0, 0, inner_v)
+
+    @pl.when(home != 1)
     def _():
         relay(3)
         fan_out(4)
 
-    gate_up(0, 1)
-
-    @pl.when(home == 0)
+    @pl.when(home == 1)
     def _():
         fan_out(3)
 
-    down(0)
-    wait_full(1)
-    gate_up(1, 0)
-
-    @pl.when(home > 0)
-    def _():
-        relay(4)
-
-    gate_up(1, 1)
-
-    @pl.when(home == 0)
-    def _():
+    gate_up(0, 1, inner_v)
+    down(0, inner_v, 4)
+
+    @pl.when(home == 1)
+    def _():
+        wait_full(own)
+        gate_up(own, 0, own_inner_v)
+        gate_up(own, 1, own_inner_v)
         relay(3)
         fan_out(4)
+        down(own, own_inner_v, 4)
+
+    wait_full(1)
+    gate_up(1, 0, inner_v)
+    relay(4)
+    gate_up(1, 1, inner_v)
+
+    @pl.when(home != 1)
+    def _():
+        gate_up(own, 1, own_inner_v)
 
     pair_up(0)
-    down(1)
+    down(1, inner_v, 4)
     wait_full(2)
-    gate_up(2, 0)
-
-    @pl.when(home == 0)
-    def _():
-        relay(4)
-
-    gate_up(2, 1)
+    gate_up(2, 0, inner_v)
+    gate_up(2, 1, inner_v)
     pair_up(1)
     finish(0)
-    down(2)
-    wait_full(3)
-    gate_up(3, 0)
-    gate_up(3, 1)
+    down(2, inner_v, 4)
+
+    @pl.when(home != 1)
+    def _():
+        down(own, own_inner_v, 2)
+
+    finish(1)
     pair_up(2)
-    finish(1)
-    down(3)
+
+    @pl.when(home != 1)
+    def _():
+        part_copy(2, own).start()
+        part_copy(3, own).start()
+
+    pair_up(own)
     finish(2)
-    pair_up(3)
-    finish(3)
+    finish(own)
 
     with scope("o_back"):
         drain(back_v.at[pl.ds(0, n_sp - 1)], back_sem.at[0])
@@ -827,7 +874,7 @@
     for q in range(4):
         out_copy(t, q, tx, min(q, 2)).start()
         out_copy(t, 3 - q, ty, min(q, 2) + (3 if q < 2 else 0)).start()
-    own_copy = pltpu.make_async_copy(final_v, out_ref.at[row_block(t)], local_sem.at[4])
+    own_copy = pltpu.make_async_copy(final_v, out_ref.at[row_block(t)], local_sem.at[17])
     own_copy.start()
     piece = final_v.at[:, pl.ds(0, width // 4)]
     with scope("q_out"):
@@ -872,15 +919,20 @@
     units = expert_gate.shape[2]
     feat = HEAD_FEATURES
     low, full = jnp.bfloat16, jnp.float32
-    vmem = pl.BlockSpec(memory_space=pltpu.VMEM)
     hbm = pl.BlockSpec(memory_space=pl.ANY)
     dma = pltpu.SemaphoreType.DMA
+    arrays = [
+        residual_in, queries, keys, values, out_gate, beta_logit, decay_logit,
+        decay_log.reshape(1, heads), head_gain.reshape(1, -1), norm_gain.reshape(1, -1),
+        final_gain.reshape(1, -1), expert_index.T, route_weights.T,
+    ]
     return pl.pallas_call(
         functools.partial(layer_kernel, n_sp, n_tp),
         out_shape=pltpu.VMEM((length, width), low),
-        in_specs=[vmem] * 13 + [hbm] * 4,
+        in_specs=[hbm] * 17,
         out_specs=hbm,
-        scratch_shapes=[
+        scratch_shapes=[pltpu.VMEM(a.shape, a.dtype) for a in arrays]
+        + [
             pltpu.VMEM(out_weight.shape, low),
             pltpu.VMEM(expert_gate.shape[1:], low),
             pltpu.VMEM(expert_up.shape[1:], low),
@@ -901,13 +953,14 @@
             pltpu.VMEM((n_sp, cap, width), low),
             pltpu.VMEM((chunks, n_tp, GROUP, cap, width), low),
             pltpu.VMEM((n_tp * GROUP * cap, units), low),
+            pltpu.VMEM((n_tp * GROUP * cap, units), low),
             pltpu.VMEM((chunks, n_tp, GROUP * cap, width), low),
             pltpu.VMEM((6, chunks, GROUP * cap, width // 2), low),
             pltpu.VMEM((2, chunks, GROUP * cap, width // 2), low),
             pltpu.VMEM((chunks, GROUP, cap, width), low),
             pltpu.VMEM((n_sp, cap, width), low),
             pltpu.VMEM((rows, width), low),
-            dma((5,)),
+            dma((18,)),
             dma((9,)),
             dma((heads,)),
             dma((heads,)),
@@ -917,19 +970,14 @@
             dma((chunks + 1, 2)),
             dma((chunks,)),
             dma((chunks, 2)),
-            dma((chunks,)),
+            dma((chunks, 2)),
             dma((1,)),
             dma((5,)),
         ],
         compiler_params=pltpu.CompilerParams(
             collective_id=0, has_side_effects=True, vmem_limit_bytes=60 * 1024 * 1024
         ),
-    )(
-        residual_in, queries, keys, values, out_gate, beta_logit, decay_logit,
-        decay_log.reshape(1, heads), head_gain.reshape(1, -1), norm_gain.reshape(1, -1),
-        final_gain.reshape(1, -1), expert_index.T, route_weights.T, out_weight, expert_gate,
-        expert_up, expert_down,
-    )
+    )(*arrays, out_weight, expert_gate, expert_up, expert_down)
 
 
 def any_size(*args):

time: 74.4 us -> 70.6 us (0.949); the launches traced: 74.3 us -> 69.4 us
  Pallas kernels: 73.5 us -> 68.6 us
    pallas_call x1, Pallas kernels: 73.5 us -> 68.6 us  [fused(): pl.pallas_call(functools.partial(layer_kernel, n_sp, n_tp), out_shape=plt...]
where the time goes in v3:
time: 70.6 us; the launch traced here: 69.4 us
  Pallas kernels  68.6 us (97%)
  local copies, waits for them, and re-layouts  0.8 us (1%)
    pallas_call x1, Pallas kernels, fused(): pl.pallas_call(functools.partial(layer_kernel, n_sp, n_tp), out_shape=plt...  68.6 us

profile of v3, /device:TPU:16, one launch (start us, length us, event | category | flops | bytes accessed | tf_op | source)
XLA Modules:
  0.0 69.4 jit_solution(16285793376186509995)
XLA Ops:
  0.0 68.6 %shard_map.163 = bf16[128,2048]{1,0:T(8,128)(2,1)S(1)} custom-call(bf16[128,2048]{1,0:T(8,128)(2,1)} %residual_hbm.1, bf16[128,512]{1,0:T(8,128)(2,1)} %query_hbm.1, bf16[128,512]{1,0:T(8,128)(2,1)} %key_hbm.1, bf16[128,512]{1,0:T(8,128)(2,1)} %value_hbm.1, bf16[128,512]{1,0:T(8,128)(2,1)} %out_gate_hbm.1, bf16[4,128]{1,0:T(4,128)(2,1)} %beta_hbm.1, ...), custom_call_target="tpu_custom_call" | custom-call | tf_op jit(solution)/shard_map/pallas_call | solution.py:929
  68.6 0.8 %copy.19 = bf16[128,2048]{1,0:T(8,128)(2,1)} copy(bf16[128,2048]{1,0:T(8,128)(2,1)S(1)} %shard_map.163) | data formatting | bytes 1048576

commit v4 on v3

--- a/solution.py
+++ b/solution.py
@@ -13,8 +13,9 @@
 TOP = 2
 BLOCK = 64
 GROUP = 2
-VISITS = ((1, 2, 3, 0), (0, 2, 3, 1), (0, 3, 1, 2), (0, 1, 2, 3))
-SENDS = ((1, 2, 3), (0, 2, 3), (3, 0, 1), (2, 0, 1))
+OUT_PARTS = 8
+VISITS = ((1, 2, 3, 0), (0, 3, 2, 1), (0, 3, 1, 2), (0, 1, 2, 3))
+SENDS = ((1, 2, 3), (0, 2, 3), (3, 0, 1), (2, 1, 0))
 
 
 highest_precision = lax.Precision.HIGHEST
@@ -818,7 +819,7 @@
         gate_up(own, 1, own_inner_v)
         relay(3)
         fan_out(4)
-        down(own, own_inner_v, 4)
+        down(own, own_inner_v, 0)
 
     wait_full(1)
     gate_up(1, 0, inner_v)
@@ -838,6 +839,11 @@
     finish(0)
     down(2, inner_v, 4)
 
+    @pl.when(home == 1)
+    def _():
+        part_copy(0, own).start()
+        part_copy(1, own).start()
+
     @pl.when(home != 1)
     def _():
         down(own, own_inner_v, 2)
@@ -845,11 +851,8 @@
     finish(1)
     pair_up(2)
 
-    @pl.when(home != 1)
-    def _():
-        part_copy(2, own).start()
-        part_copy(3, own).start()
-
+    part_copy(2, own).start()
+    part_copy(3, own).start()
     pair_up(own)
     finish(2)
     finish(own)
@@ -858,31 +861,34 @@
         drain(back_v.at[pl.ds(0, n_sp - 1)], back_sem.at[0])
 
     back = back_v[...].reshape(slots, width)
+    chosen = mm(jnp.concatenate(tables, 0), back)
     routed = jnp.zeros((rows, width), jnp.float32)
     for j in range(TOP):
-        routed = routed + weights[:, j : j + 1] * mm(tables[j], back)
+        routed = routed + weights[:, j : j + 1] * chosen[j * rows : (j + 1) * rows]
     final_v[...] = layer_norm(
         residual_scale * hidden_v[...].astype(jnp.float32) + routed, final_gain_ref[...]
     ).astype(jnp.bfloat16)
 
     def out_copy(owner, q, to, sem):
-        cols = pl.ds(q * (width // 4), width // 4)
+        cols = pl.ds(q * (width // OUT_PARTS), width // OUT_PARTS)
         cells = out_ref.at[row_block(owner), cols]
         source = final_v.at[:, cols] if owner is t else cells
         return remote(source, cells, sent_sem.at[8], out_sem.at[sem], s, to)
 
-    for q in range(4):
-        out_copy(t, q, tx, min(q, 2)).start()
-        out_copy(t, 3 - q, ty, min(q, 2) + (3 if q < 2 else 0)).start()
+    early = OUT_PARTS // 2
+    for q in range(OUT_PARTS):
+        rest = 2 * early
+        out_copy(t, q, tx, q if q < early else rest).start()
+        out_copy(t, OUT_PARTS - 1 - q, ty, early + q if q < early else rest).start()
     own_copy = pltpu.make_async_copy(final_v, out_ref.at[row_block(t)], local_sem.at[17])
     own_copy.start()
-    piece = final_v.at[:, pl.ds(0, width // 4)]
+    piece = final_v.at[:, pl.ds(0, width // OUT_PARTS)]
     with scope("q_out"):
-        for q in range(2):
+        for q in range(early):
             drain(piece, out_sem.at[q])
-            out_copy(tx, q, ty, 2).start()
-            drain(piece, out_sem.at[3 + q])
-            out_copy(ty, 3 - q, tx, 2).start()
+            out_copy(tx, q, ty, 2 * early).start()
+            drain(piece, out_sem.at[early + q])
+            out_copy(ty, OUT_PARTS - 1 - q, tx, 2 * early).start()
 
     @pl.when(core == 0)
     def _():
@@ -903,7 +909,7 @@
     drain(back_v.at[pl.ds(0, n_sp - 1)], sent_sem.at[7])
     own_copy.wait()
     with scope("r_out"):
-        drain(proj_in.at[pl.ds(0, 2)], out_sem.at[2])
+        drain(proj_in.at[pl.ds(0, 2)], out_sem.at[OUT_PARTS])
     with scope("s_sends"):
         drain(proj_in, sent_sem.at[8])
 
@@ -972,7 +978,7 @@
             dma((chunks, 2)),
             dma((chunks, 2)),
             dma((1,)),
-            dma((5,)),
+            dma((OUT_PARTS + 1,)),
         ],
         compiler_params=pltpu.CompilerParams(
             collective_id=0, has_side_effects=True, vmem_limit_bytes=60 * 1024 * 1024
@@ -994,7 +1000,8 @@
         and cap % 16 == 0
         and (length // n_tp) % 16 == 0
         and (n_sp * cap) % 128 == 0
-        and width % 512 == 0
+        and width % 1024 == 0
+        and width % (128 * OUT_PARTS) == 0
         and expert_gate.shape[2] % 256 == 0
     )
     return fused(args, n_sp, n_tp, cap) if fits else per_device(*args)

time: 70.6 us -> 69.4 us (0.983); the launches traced: 69.4 us -> 69.3 us
  no operation moved by 1% of the time
where the time goes in v4:
time: 69.4 us; the launch traced here: 69.3 us
  Pallas kernels  68.5 us (99%)
  local copies, waits for them, and re-layouts  0.8 us (1%)
    pallas_call x1, Pallas kernels, fused(): pl.pallas_call(functools.partial(layer_kernel, n_sp, n_tp), out_shape=plt...  68.5 us

profile of v4, /device:TPU:16, one launch (start us, length us, event | category | flops | bytes accessed | tf_op | source)
XLA Modules:
  0.0 69.3 jit_solution(8243298253229211723)
XLA Ops:
  0.0 68.5 %shard_map.163 = bf16[128,2048]{1,0:T(8,128)(2,1)S(1)} custom-call(bf16[128,2048]{1,0:T(8,128)(2,1)} %residual_hbm.1, bf16[128,512]{1,0:T(8,128)(2,1)} %query_hbm.1, bf16[128,512]{1,0:T(8,128)(2,1)} %key_hbm.1, bf16[128,512]{1,0:T(8,128)(2,1)} %value_hbm.1, bf16[128,512]{1,0:T(8,128)(2,1)} %out_gate_hbm.1, bf16[4,128]{1,0:T(4,128)(2,1)} %beta_hbm.1, ...), custom_call_target="tpu_custom_call" | custom-call | tf_op jit(solution)/shard_map/pallas_call | solution.py:935
  68.5 0.8 %copy.19 = bf16[128,2048]{1,0:T(8,128)(2,1)} copy(bf16[128,2048]{1,0:T(8,128)(2,1)S(1)} %shard_map.163) | data formatting | bytes 1048576

commit v5 on v4

--- a/solution.py
+++ b/solution.py
@@ -585,8 +585,9 @@
         ).astype(jnp.bfloat16)
         return carry
 
-    for part, cols in enumerate((left, right)):
-        steps = half // 512
+    for part in range(4):
+        steps = width // 512 // 4
+        cols = slice(part * width // 4, (part + 1) * width // 4)
         with scope("d_project"):
             lax.fori_loop(part * steps, (part + 1) * steps, project, 0)
         for k in range(1, n_tp):
@@ -1000,7 +1001,7 @@
         and cap % 16 == 0
         and (length // n_tp) % 16 == 0
         and (n_sp * cap) % 128 == 0
-        and width % 1024 == 0
+        and width % 2048 == 0
         and width % (128 * OUT_PARTS) == 0
         and expert_gate.shape[2] % 256 == 0
     )

time: 69.4 us -> 69.3 us (level)
  no operation moved by 1% of the time
where the time goes in v5:
time: 69.3 us; the launch traced here: 69.2 us
  Pallas kernels  68.4 us (99%)
  local copies, waits for them, and re-layouts  0.8 us (1%)
    pallas_call x1, Pallas kernels, fused(): pl.pallas_call(functools.partial(layer_kernel, n_sp, n_tp), out_shape=plt...  68.4 us

profile of v5, /device:TPU:16, one launch (start us, length us, event | category | flops | bytes accessed | tf_op | source)
XLA Modules:
  0.0 69.2 jit_solution(14404496463467442172)
XLA Ops:
  0.0 68.4 %shard_map.163 = bf16[128,2048]{1,0:T(8,128)(2,1)S(1)} custom-call(bf16[128,2048]{1,0:T(8,128)(2,1)} %residual_hbm.1, bf16[128,512]{1,0:T(8,128)(2,1)} %query_hbm.1, bf16[128,512]{1,0:T(8,128)(2,1)} %key_hbm.1, bf16[128,512]{1,0:T(8,128)(2,1)} %value_hbm.1, bf16[128,512]{1,0:T(8,128)(2,1)} %out_gate_hbm.1, bf16[4,128]{1,0:T(4,128)(2,1)} %beta_hbm.1, ...), custom_call_target="tpu_custom_call" | custom-call | tf_op jit(solution)/shard_map/pallas_call | solution.py:936
  68.4 0.8 %copy.19 = bf16[128,2048]{1,0:T(8,128)(2,1)} copy(bf16[128,2048]{1,0:T(8,128)(2,1)S(1)} %shard_map.163) | data formatting | bytes 1048576
